TPU v7x, 32 devices: a whole 2x2x4 slice. The times are simulated.
32 devices in a mesh: grp: 2 (over y), tp: 4 (over z), dp: 4 (over x, core).
Axes of the slice: x: 2, y: 2, z: 4, core: 2. Of those that a mesh axis runs over, the one named last changes fastest.
Arguments:
- tokens: bfloat16 [256, 4096], P(('grp', 'tp'), 'dp'), parts along dimension 0, may hold values from -6 to 6
- lengths: int32 [64], P(('grp', 'dp')), parts along dimension 0, may hold values from 1 to 4, as said below
- norm_gain: float32 [2, 4096], P(None, 'dp'), may hold values from 0.1 to 1.9
- w_recept: bfloat16 [2, 4096, 2048], P(None, 'dp', 'tp'), may hold values from -0.09375 to 0.09375
- w_keys: bfloat16 [2, 4096, 2048], P(None, 'dp', 'tp'), may hold values from -0.09375 to 0.09375
- w_values: bfloat16 [2, 4096, 2048], P(None, 'dp', 'tp'), may hold values from -0.09375 to 0.09375
- w_decay: bfloat16 [2, 4096, 2048], P(None, 'dp', 'tp'), may hold values from -0.09375 to 0.09375
- w_rate: bfloat16 [2, 4096, 2048], P(None, 'dp', 'tp'), may hold values from -0.09375 to 0.09375
- w_gate: bfloat16 [2, 4096, 2048], P(None, 'dp', 'tp'), may hold values from -0.09375 to 0.09375
- decay_base: float32 [2, 2048], P(None, 'tp'), may hold values from -3 to 1
- group_gain: float32 [2, 2048], P(None, 'tp'), may hold values from 0.1 to 1.9
- w_out: bfloat16 [2, 2048, 4096], P(None, 'tp', 'dp'), may hold values from -0.125 to 0.125
- states: float32 [2, 64, 32, 4096], P(None, ('grp', 'dp'), 'tp'), parts along dimension 1, may hold values from -2 to 2
Outputs:
- tokens_out: bfloat16 [256, 4096], P(('grp', 'tp'), 'dp'), parts along dimension 0
- states_out: float32 [2, 64, 32, 4096], P(None, ('grp', 'dp'), 'tp'), parts along dimension 1
There are 2 independent parts, one for each index of `grp`. A program takes and returns all parts, laid end to end along the dimension named above; an argument that names none is the same for every part. Nothing has to cross between parts.
Inputs may be any that keep to these rules, and one draw needn't show every extreme that they name: Sequence s has its first lengths[s] of its 4 slots live; in every draw all 8 sequences of some index of dp have 4 live slots.
All inputs are finite; a program needn't handle non-finite values.
Results may differ from a plain program's by a relative error of at most 0.029.
Values may be sent and summed in bfloat16 or wider, within the bound.
A program may use at most 128 MiB of HBM per device.

v0:
```python
import functools

import jax
import jax.numpy as jnp
from jax import lax
from jax.experimental import pallas as pl
from jax.experimental.pallas import tpu as pltpu
from jax.sharding import PartitionSpec as P

HEAD = 64
LANES = 2 * HEAD
NEW = 4
ROLES = 6
norm_epsilon = 1e-06
unit_epsilon = 0.00064
group_epsilon = 0.00064
MESH = pl.DeviceIdType.MESH
f32 = jnp.float32
bf16 = jnp.bfloat16


def kernel(
    tp_n,
    dp_n,
    model_width,
    tokens,
    lengths,
    norm_gain,
    w_recept,
    w_keys,
    w_values,
    w_decay,
    w_rate,
    w_gate,
    decay_base,
    group_gain,
    w_out,
    states,
    tokens_out,
    states_out,
    gat,
    gain_vm,
    base_vm,
    group_vm,
    w_vm,
    wo_vm,
    st_vm,
    so_vm,
    expand,
    scaled,
    part,
    pair,
    csend,
    crecv,
    sq_part,
    sq_pair,
    sq_send,
    sq_recv,
    yscr,
    rel,
    rows_base,
    rows_gain,
    rows_len,
    prod,
    mixrel,
    mixf,
    mixed,
    psend,
    precv,
    ship,
    load_sem,
    w_sem,
    store_sem,
    gat_s,
    gat_r,
    pair_s,
    pair_r,
    cs_s,
    cs_r,
    mix_s,
    mix_r,
    p_s,
    p_r,
):
    g = lax.axis_index("grp")
    t = lax.axis_index("tp")
    d = lax.axis_index("dp")
    chips = dp_n // 2
    x = d // 2
    c = lax.rem(d, 2)
    local, feat = tokens.shape
    total = local * tp_n
    own = total // dp_n
    width = w_recept.shape[2]
    heads = width // HEAD
    seqs = own // NEW
    rows = seqs * heads
    flat = states.shape[2]

    own_gat = gat.at[0, pl.ds(pl.multiple_of(t * local, local), local)]
    loads = [
        pltpu.make_async_copy(tokens, own_gat, load_sem.at[0]),
        pltpu.make_async_copy(norm_gain, gain_vm, load_sem.at[1]),
        pltpu.make_async_copy(decay_base, base_vm, load_sem.at[2]),
        pltpu.make_async_copy(group_gain, group_vm, load_sem.at[3]),
    ]
    for copy in loads:
        copy.start()
    weights = (w_recept, w_keys, w_values, w_decay, w_rate, w_gate)
    w_loads, wo_loads, st_loads = [], [], []
    for b in range(2):
        w_loads.append(
            [
                pltpu.make_async_copy(weights[r].at[b], w_vm.at[b, r], w_sem.at[b, r])
                for r in range(ROLES)
            ]
        )
        st_loads.append(pltpu.make_async_copy(states.at[b], st_vm.at[b], w_sem.at[b, ROLES]))
        wo_loads.append(pltpu.make_async_copy(w_out.at[b], wo_vm.at[b], w_sem.at[b, ROLES + 1]))
        for copy in w_loads[b]:
            copy.start()
        st_loads[b].start()
        wo_loads[b].start()

    def tp_peer(o):
        return (g, lax.rem(t + o, tp_n), d)

    def dp_peer(o):
        return (g, t, lax.rem(d + o, dp_n))

    sibling = (g, t, x * 2 + 1 - c)

    def chip_peer(o):
        return (g, t, lax.rem(x + o, chips) * 2 + c)

    barrier = pltpu.get_barrier_semaphore()
    for o in range(1, tp_n):
        pl.semaphore_signal(barrier, inc=1, device_id=tp_peer(o), device_id_type=MESH)
    for o in range(1, dp_n):
        pl.semaphore_signal(barrier, inc=1, device_id=dp_peer(o), device_id_type=MESH)
    pl.semaphore_wait(barrier, tp_n - 1 + dp_n - 1)

    def remote(src, dst, ss, rs, dev):
        return pltpu.make_async_remote_copy(
            src_ref=src, dst_ref=dst, send_sem=ss, recv_sem=rs, device_id=dev, device_id_type=MESH
        )

    pending = []

    def gather_tokens(b):
        mine = gat.at[b, pl.ds(pl.multiple_of(t * local, local), local)]
        copies = [
            remote(mine, mine, gat_s.at[b, o], gat_r.at[b, o], tp_peer(o)) for o in range(1, tp_n)
        ]
        for copy in copies:
            copy.start()
        pending.extend(copies)
        return copies

    loads[0].wait()
    arrivals = gather_tokens(0)
    for copy in loads[1:]:
        copy.wait()

    lane = lax.broadcasted_iota(jnp.int32, (seqs, LANES), 1)
    low = lane < HEAD

    chunk = 512
    for i in range(flat // chunk):
        r_id = lax.broadcasted_iota(jnp.int32, (chunk, LANES), 0) + i * chunk
        c_id = lax.broadcasted_iota(jnp.int32, (chunk, LANES), 1)
        expand[pl.ds(i * chunk, chunk), :] = jnp.where(
            (r_id // HEAD) == lax.rem(c_id, HEAD), 1.0, 0.0
        ).astype(bf16)
    for b in range(2):
        for src, dst in ((base_vm, rows_base), (group_vm, rows_gain)):
            for hp in range(heads // 2):
                a = jnp.broadcast_to(src[b : b + 1, hp * LANES : (hp + 1) * LANES], (seqs, LANES))
                turned = pltpu.roll(a, HEAD, 1)
                dst[b, pl.ds(2 * hp, seqs, stride=heads), :] = jnp.where(low, a, turned)
                dst[b, pl.ds(2 * hp + 1, seqs, stride=heads), :] = jnp.where(low, turned, a)
    for s in range(seqs):
        rows_len[s * heads : (s + 1) * heads, :] = jnp.full(
            (heads, LANES), lengths[s].astype(f32), f32
        )

    for b in range(2):
        for copy in arrivals:
            copy.wait_recv()
        wide = gat[b].astype(f32)
        scaled[...] = (wide * gain_vm[b : b + 1, :]).astype(bf16)
        square = jnp.broadcast_to(jnp.sum(wide * wide, 1, keepdims=True), (total, LANES))
        sq_part[b] = square.reshape(chips, 2, own, LANES)

        def to_sibling(src, dst, i):
            copy = remote(
                src.at[:, 1 - c], dst, pair_s.at[b, i], pair_r.at[b, i], sibling
            )
            copy.start()
            pending.append(copy)
            return copy

        def to_chips(src, dst, i):
            copies = []
            for o in range(1, chips):
                copy = remote(
                    src.at[lax.rem(x + o, chips)],
                    dst.at[o],
                    cs_s.at[b, i, o],
                    cs_r.at[b, i, o],
                    chip_peer(o),
                )
                copy.start()
                copies.append(copy)
            pending.extend(copies)
            return copies

        pair_copies = [to_sibling(sq_part.at[b], sq_pair.at[b], ROLES)]
        chip_copies = []

        def forward_square():
            pair_copies[0].wait_recv()
            for o in range(1, chips):
                xx = lax.rem(x + o, chips)
                sq_send[b, xx] = sq_part[b, xx, c] + sq_pair[b, xx]
            chip_copies.append(to_chips(sq_send.at[b], sq_recv.at[b], ROLES))

        def forward(r):
            pair_copies[r + 1].wait_recv()
            for o in range(1, chips):
                xx = lax.rem(x + o, chips)
                csend[b, r, xx] = (
                    part[b, r, xx, c].astype(f32) + pair[b, r, xx].astype(f32)
                ).astype(bf16)
            chip_copies.append(to_chips(csend.at[b, r], crecv.at[b, r], r))

        for r in range(ROLES):
            w_loads[b][r].wait()
            y = jnp.dot(scaled[...], w_vm[b, r], preferred_element_type=f32)
            part[b, r] = y.astype(bf16).reshape(chips, 2, own, width)
            pair_copies.append(to_sibling(part.at[b, r], pair.at[b, r], r))
            if r == 0:
                forward_square()
            else:
                forward(r - 1)
        forward(ROLES - 1)

        for copy in chip_copies[0]:
            copy.wait_recv()
        square = sq_part[b, x, c] + sq_pair[b, x]
        for o in range(1, chips):
            square = square + sq_recv[b, o]
        inv_rms = lax.rsqrt(square[:, :1] / model_width + norm_epsilon)

        for r in range(ROLES):
            for copy in chip_copies[r + 1]:
                copy.wait_recv()
            y = part[b, r, x, c].astype(f32) + pair[b, r, x].astype(f32)
            for o in range(1, chips):
                y = y + crecv[b, r, o].astype(f32)
            y = (inv_rms * y).astype(bf16).astype(f32)
            for hp in range(heads // 2):
                yscr[r, hp] = y[:, hp * LANES : (hp + 1) * LANES]
            for n in range(NEW):
                for hp in range(heads // 2):
                    a = yscr[r, hp, pl.ds(n, seqs, stride=NEW), :]
                    turned = pltpu.roll(a, HEAD, 1)
                    rel[r * NEW + n, pl.ds(2 * hp, seqs, stride=heads), :] = jnp.where(
                        low, a, turned
                    )
                    rel[r * NEW + n, pl.ds(2 * hp + 1, seqs, stride=heads), :] = jnp.where(
                        low, turned, a
                    )

        def half_sum(z):
            return 0.5 * jnp.sum(z, 1, keepdims=True)

        st_loads[b].wait()
        carried = None
        units, cs, ks, qs, vs, ws, vecs_u, vecs_q, lives = [], [], [], [], [], [], [], [], []
        for n in range(NEW):
            q, k, v, dec, rate = [rel[r * NEW + n] for r in range(5)]
            live = jnp.where(rows_len[...] > n + 0.5, 1.0, 0.0)
            w = jnp.exp(-jnp.exp(-jax.nn.softplus(-(rows_base[b] + dec)) - 0.5))
            w = jnp.where(live > 0.5, w, 1.0)
            u = k * lax.rsqrt(half_sum(k * k) + unit_epsilon)
            units.append(u)
            cs.append(live * (u * jax.nn.sigmoid(rate)))
            ks.append(live * k)
            qs.append(q)
            vs.append(v)
            ws.append(w)
            lives.append(live)
            vecs_u.append(u if carried is None else carried * u)
            carried = w if carried is None else carried * w
            vecs_q.append(carried * q)
        for j in range(flat // LANES):
            s0 = st_vm[b, :, j * LANES : (j + 1) * LANES]
            for i, vec in enumerate(vecs_u + vecs_q):
                prod[i * rows : (i + 1) * rows, j * LANES : (j + 1) * LANES] = (s0 * vec).astype(
                    bf16
                )
        reads = jnp.dot(prod[...], expand[...], preferred_element_type=f32)
        ps, ct, kt = [], [], []
        for n in range(NEW):
            p = reads[n * rows : (n + 1) * rows]
            for j in range(n):
                p = p - ps[j] * half_sum(ct[j] * units[n]) + vs[j] * half_sum(kt[j] * units[n])
            ps.append(p)
            ct = [z * ws[n] for z in ct] + [cs[n]]
            kt = [z * ws[n] for z in kt] + [ks[n]]
            o_n = reads[(NEW + n) * rows : (NEW + n + 1) * rows]
            for j in range(n + 1):
                o_n = o_n - ps[j] * half_sum(ct[j] * qs[n]) + vs[j] * half_sum(kt[j] * qs[n])
            mean = jnp.mean(o_n, 1, keepdims=True)
            off = o_n - mean
            var = jnp.mean(off * off, 1, keepdims=True)
            normed = off * lax.rsqrt(var + group_epsilon) * rows_gain[b]
            mixrel[n] = lives[n] * jax.nn.sigmoid(rel[5 * NEW + n]) * normed
            for hp in range(heads // 2):
                even = mixrel[n, pl.ds(2 * hp, seqs, stride=heads), :]
                odd = mixrel[n, pl.ds(2 * hp + 1, seqs, stride=heads), :]
                mixf[hp, pl.ds(n, seqs, stride=NEW), :] = jnp.where(low, even, odd)
        for hp in range(heads // 2):
            mixed[
                b, pl.ds(pl.multiple_of(d * own, own), own), hp * LANES : (hp + 1) * LANES
            ] = mixf[hp].astype(bf16)
        mine = mixed.at[b, pl.ds(pl.multiple_of(d * own, own), own)]
        mix_copies = [
            remote(mine, mine, mix_s.at[b, o], mix_r.at[b, o], dp_peer(o)) for o in range(1, dp_n)
        ]
        for copy in mix_copies:
            copy.start()
        pending.extend(mix_copies)

        wide_lane = lax.broadcasted_iota(jnp.int32, (rows, LANES), 1) < HEAD
        for i in range(NEW):
            ship[2 * i * rows : (2 * i + 1) * rows, :] = jnp.where(wide_lane, -ps[i], 0.0).astype(
                bf16
            )
            ship[(2 * i + 1) * rows : (2 * i + 2) * rows, :] = jnp.where(
                wide_lane, vs[i], 0.0
            ).astype(bf16)
        step = 512
        for j in range(flat // step):
            spread = lax.dot_general(
                ship[...],
                expand[j * step : (j + 1) * step, :],
                (((1,), (1,)), ((), ())),
                preferred_element_type=f32,
            )
            for m in range(step // LANES):
                lanes = slice(m * LANES, (m + 1) * LANES)
                at = slice(j * step + m * LANES, j * step + (m + 1) * LANES)
                acc = st_vm[b, :, at] * carried
                for i in range(NEW):
                    acc = acc + spread[2 * i * rows : (2 * i + 1) * rows, lanes] * ct[i]
                    acc = acc + spread[(2 * i + 1) * rows : (2 * i + 2) * rows, lanes] * kt[i]
                so_vm[b, :, at] = acc
        pltpu.make_async_copy(so_vm.at[b], states_out.at[b], store_sem.at[b]).start()

        for copy in mix_copies:
            copy.wait_recv()
        wo_loads[b].wait()
        outp = jnp.dot(mixed[b], wo_vm[b], preferred_element_type=f32)
        psend[b] = outp.astype(bf16).reshape(tp_n, local, feat)
        p_copies = []
        for o in range(1, tp_n):
            copy = remote(
                psend.at[b, lax.rem(t + o, tp_n)],
                precv.at[b, o],
                p_s.at[b, o],
                p_r.at[b, o],
                tp_peer(o),
            )
            copy.start()
            p_copies.append(copy)
        pending.extend(p_copies)
        here = pl.ds(pl.multiple_of(t * local, local), local)
        acc = psend[b, t].astype(f32)
        for o in range(1, tp_n):
            p_copies[o - 1].wait_recv()
            acc = acc + precv[b, o].astype(f32)
        fresh = (gat[b, here, :].astype(f32) + acc).astype(bf16)
        if b == 0:
            gat[1, here, :] = fresh
            arrivals = gather_tokens(1)
        else:
            tokens_out[...] = fresh

    for b in range(2):
        pltpu.make_async_copy(so_vm.at[b], states_out.at[b], store_sem.at[b]).wait()
    for copy in pending:
        copy.wait_send()


def solution(mesh):
    tp_n = mesh.shape["tp"]
    dp_n = mesh.shape["dp"]
    chips = dp_n // 2

    def per_device(*args):
        tokens, lengths = args[0], args[1]
        w_recept, w_out, states = args[3], args[11], args[12]
        local, feat = tokens.shape
        total = local * tp_n
        own = total // dp_n
        width = w_recept.shape[2]
        heads = width // HEAD
        seqs = lengths.shape[0]
        rows = seqs * heads
        flat = states.shape[3]
        flat_states = states.reshape(2, rows, flat)
        any_spec = pl.BlockSpec(memory_space=pl.ANY)
        vmem = pltpu.VMEM
        dma = pltpu.SemaphoreType.DMA
        tokens_out, states_out = pl.pallas_call(
            functools.partial(kernel, tp_n, dp_n, feat * dp_n),
            out_shape=(
                jax.ShapeDtypeStruct((local, feat), bf16),
                jax.ShapeDtypeStruct((2, rows, flat), f32),
            ),
            in_specs=[any_spec, pl.BlockSpec(memory_space=pltpu.SMEM)] + [any_spec] * 11,
            out_specs=(pl.BlockSpec(memory_space=pltpu.VMEM), any_spec),
            scratch_shapes=[
                vmem((2, total, feat), bf16),
                vmem((2, feat), f32),
                vmem((2, width), f32),
                vmem((2, width), f32),
                vmem((2, ROLES, feat, width), bf16),
                vmem((2, width, feat), bf16),
                vmem((2, rows, flat), f32),
                vmem((2, rows, flat), f32),
                vmem((flat, LANES), bf16),
                vmem((total, feat), bf16),
                vmem((2, ROLES, chips, 2, own, width), bf16),
                vmem((2, ROLES, chips, own, width), bf16),
                vmem((2, ROLES, chips, own, width), bf16),
                vmem((2, ROLES, chips, own, width), bf16),
                vmem((2, chips, 2, own, LANES), f32),
                vmem((2, chips, own, LANES), f32),
                vmem((2, chips, own, LANES), f32),
                vmem((2, chips, own, LANES), f32),
                vmem((ROLES, heads // 2, own, LANES), f32),
                vmem((ROLES * NEW, rows, LANES), f32),
                vmem((2, rows, LANES), f32),
                vmem((2, rows, LANES), f32),
                vmem((rows, LANES), f32),
                vmem((2 * NEW * rows, flat), bf16),
                vmem((NEW, rows, LANES), f32),
                vmem((heads // 2, own, LANES), f32),
                vmem((2, total, width), bf16),
                vmem((2, tp_n, local, feat), bf16),
                vmem((2, tp_n, local, feat), bf16),
                vmem((2 * NEW * rows, LANES), bf16),
                dma((4,)),
                dma((2, ROLES + 2)),
                dma((2,)),
                dma((2, tp_n)),
                dma((2, tp_n)),
                dma((2, ROLES + 1)),
                dma((2, ROLES + 1)),
                dma((2, ROLES + 1, chips)),
                dma((2, ROLES + 1, chips)),
                dma((2, dp_n)),
                dma((2, dp_n)),
                dma((2, tp_n)),
                dma((2, tp_n)),
            ],
            compiler_params=pltpu.CompilerParams(
                collective_id=0, has_side_effects=True, vmem_limit_bytes=60 * 1024 * 1024
            ),
        )(*args[:12], flat_states)
        return tokens_out, states_out.reshape(states.shape)

    placed = (
        P(("grp", "tp"), "dp"),
        P(("grp", "dp")),
        P(None, "dp"),
        P(None, "dp", "tp"),
        P(None, "dp", "tp"),
        P(None, "dp", "tp"),
        P(None, "dp", "tp"),
        P(None, "dp", "tp"),
        P(None, "dp", "tp"),
        P(None, "tp"),
        P(None, "tp"),
        P(None, "tp", "dp"),
        P(None, ("grp", "dp"), "tp", None),
    )
    return jax.shard_map(
        per_device,
        mesh=mesh,
        in_specs=placed,
        out_specs=(P(("grp", "tp"), "dp"), P(None, ("grp", "dp"), "tp", None)),
        check_vma=False,
    )
```

profile of v0, /device:TPU:0, one launch (start us, length us, event | category | flops | bytes accessed | tf_op | source)
XLA Modules:
  0.0 71.9 jit_solution(5164555967466567136)
XLA Ops:
  0.6 66.7 %shard_map.140 = (bf16[32,1024]{1,0:T(8,128)(2,1)}, f32[2,64,4096]{2,1,0:T(8,128)}) custom-call(bf16[32,1024]{1,0:T(8,128)(2,1)} %tokens.1, s32[8]{0:T(128)} %lengths.1, f32[2,1024]{1,0:T(2,128)} %norm_gain.1, bf16[2,1024,512]{2,1,0:T(8,128)(2,1)} %w_recept.1, bf16[2,1024,512]{2,1,0:T(8,128)(2,1)} %w_keys.1, bf16[2,1024,512]{2,1,0:T(8,128)(2,1)} %w_values.1, ...), custom_call_target="tpu_custom_call" | custom-call | tf_op jit(solution)/shard_map/pallas_call | solution.py:417
  67.3 1.5 %copy.17 = bf16[32,1024]{1,0:T(8,128)(2,1)} copy(bf16[32,1024]{1,0:T(8,128)(2,1)} %get-tuple-element.8) | data formatting | bytes 131072
  68.8 3.1 %copy.18 = f32[2,8,8,4096]{3,2,1,0:T(8,128)} copy(f32[2,8,8,4096]{3,2,1,0:T(8,128)} %bitcast.2) | data formatting | bytes 4194304
where the time goes:
time: 72.1 us; the launch traced here: 71.9 us
  Pallas kernels  66.7 us (93%)
  local copies, waits for them, and re-layouts  4.58 us (6%)
    pallas_call x1, Pallas kernels, per_device(): pl.pallas_call(functools.partial(kernel, tp_n, dp_n, feat * dp_n), out_sh...  66.7 us
    unnamed x2, local copies, waits for them, and re-layouts  4.58 us

commit v1 on v0

--- a/solution.py
+++ b/solution.py
@@ -68,6 +68,11 @@
     psend,
     precv,
     ship,
+    factors,
+    run,
+    came,
+    run_s,
+    run_r,
     load_sem,
     w_sem,
     store_sem,
@@ -106,7 +111,7 @@
     ]
     for copy in loads:
         copy.start()
-    weights = (w_recept, w_keys, w_values, w_decay, w_rate, w_gate)
+    weights = (w_keys, w_decay, w_recept, w_rate, w_values, w_gate)
     w_loads, wo_loads, st_loads = [], [], []
     for b in range(2):
         w_loads.append(
@@ -184,9 +189,48 @@
             (heads, LANES), lengths[s].astype(f32), f32
         )
 
+    half = local // 2
+    step = 512
+    early = (3, 3)
+
+    @pl.when(t == 0)
+    def _():
+        came[0] = jnp.zeros(came.shape[1:], bf16)
+
+    @pl.when(t == tp_n - 1)
+    def _():
+        came[1] = jnp.zeros(came.shape[1:], bf16)
+
+    def half_sum(z):
+        return 0.5 * jnp.sum(z, 1, keepdims=True)
+
+    def new_state(b, start, stop):
+        for j in range(start, stop):
+            spread = lax.dot_general(
+                ship[b],
+                expand[j * step : (j + 1) * step, :],
+                (((1,), (1,)), ((), ())),
+                preferred_element_type=f32,
+            )
+            for m in range(step // LANES):
+                lanes = slice(m * LANES, (m + 1) * LANES)
+                at = slice(j * step + m * LANES, j * step + (m + 1) * LANES)
+                acc = st_vm[b, :, at] * factors[b, 0]
+                for i in range(NEW):
+                    acc = (
+                        acc
+                        + spread[2 * i * rows : (2 * i + 1) * rows, lanes] * factors[b, 1 + i]
+                        + spread[(2 * i + 1) * rows : (2 * i + 2) * rows, lanes]
+                        * factors[b, 1 + NEW + i]
+                    )
+                so_vm[b, :, at] = acc
+        if stop == flat // step:
+            pltpu.make_async_copy(so_vm.at[b], states_out.at[b], store_sem.at[b]).start()
+
     for b in range(2):
-        for copy in arrivals:
-            copy.wait_recv()
+        if b == 0:
+            for copy in arrivals:
+                copy.wait_recv()
         wide = gat[b].astype(f32)
         scaled[...] = (wide * gain_vm[b : b + 1, :]).astype(bf16)
         square = jnp.broadcast_to(jnp.sum(wide * wide, 1, keepdims=True), (total, LANES))
@@ -252,7 +296,7 @@
             square = square + sq_recv[b, o]
         inv_rms = lax.rsqrt(square[:, :1] / model_width + norm_epsilon)
 
-        for r in range(ROLES):
+        def receive(r):
             for copy in chip_copies[r + 1]:
                 copy.wait_recv()
             y = part[b, r, x, c].astype(f32) + pair[b, r, x].astype(f32)
@@ -271,52 +315,69 @@
                     rel[r * NEW + n, pl.ds(2 * hp + 1, seqs, stride=heads), :] = jnp.where(
                         low, turned, a
                     )
-
-        def half_sum(z):
-            return 0.5 * jnp.sum(z, 1, keepdims=True)
+            return [rel[r * NEW + n] for n in range(NEW)]
+
+        def read_state(vecs):
+            for j in range(flat // LANES):
+                s0 = st_vm[b, :, j * LANES : (j + 1) * LANES]
+                for i, vec in enumerate(vecs):
+                    prod[i * rows : (i + 1) * rows, j * LANES : (j + 1) * LANES] = (
+                        s0 * vec
+                    ).astype(bf16)
+            return jnp.dot(prod[...], expand[...], preferred_element_type=f32)
 
         st_loads[b].wait()
+        keys = receive(0)
+        decs = receive(1)
+        lives, ws, units, ks, vecs, carry = [], [], [], [], [], []
         carried = None
-        units, cs, ks, qs, vs, ws, vecs_u, vecs_q, lives = [], [], [], [], [], [], [], [], []
         for n in range(NEW):
-            q, k, v, dec, rate = [rel[r * NEW + n] for r in range(5)]
             live = jnp.where(rows_len[...] > n + 0.5, 1.0, 0.0)
-            w = jnp.exp(-jnp.exp(-jax.nn.softplus(-(rows_base[b] + dec)) - 0.5))
+            w = jnp.exp(-jnp.exp(-jax.nn.softplus(-(rows_base[b] + decs[n])) - 0.5))
             w = jnp.where(live > 0.5, w, 1.0)
+            k = keys[n]
             u = k * lax.rsqrt(half_sum(k * k) + unit_epsilon)
+            lives.append(live)
             units.append(u)
-            cs.append(live * (u * jax.nn.sigmoid(rate)))
             ks.append(live * k)
-            qs.append(q)
-            vs.append(v)
             ws.append(w)
-            lives.append(live)
-            vecs_u.append(u if carried is None else carried * u)
+            vecs.append(u if carried is None else carried * u)
             carried = w if carried is None else carried * w
-            vecs_q.append(carried * q)
-        for j in range(flat // LANES):
-            s0 = st_vm[b, :, j * LANES : (j + 1) * LANES]
-            for i, vec in enumerate(vecs_u + vecs_q):
-                prod[i * rows : (i + 1) * rows, j * LANES : (j + 1) * LANES] = (s0 * vec).astype(
-                    bf16
-                )
-        reads = jnp.dot(prod[...], expand[...], preferred_element_type=f32)
-        ps, ct, kt = [], [], []
+            carry.append(carried)
+        reads_u = read_state(vecs)
+        qs = receive(2)
+        reads_q = read_state([carry[n] * qs[n] for n in range(NEW)])
+        rates = receive(3)
+        cs = [lives[n] * (units[n] * jax.nn.sigmoid(rates[n])) for n in range(NEW)]
+        ct, kt, u_c, u_k, q_c, q_k = [], [], [], [], [], []
         for n in range(NEW):
-            p = reads[n * rows : (n + 1) * rows]
-            for j in range(n):
-                p = p - ps[j] * half_sum(ct[j] * units[n]) + vs[j] * half_sum(kt[j] * units[n])
-            ps.append(p)
+            u_c.append([half_sum(z * units[n]) for z in ct])
+            u_k.append([half_sum(z * units[n]) for z in kt])
             ct = [z * ws[n] for z in ct] + [cs[n]]
             kt = [z * ws[n] for z in kt] + [ks[n]]
-            o_n = reads[(NEW + n) * rows : (NEW + n + 1) * rows]
+            q_c.append([half_sum(z * qs[n]) for z in ct])
+            q_k.append([half_sum(z * qs[n]) for z in kt])
+        factors[b, 0] = carried
+        for n in range(NEW):
+            factors[b, 1 + n] = ct[n]
+            factors[b, 1 + NEW + n] = kt[n]
+        vs = receive(4)
+        ps, outs = [], []
+        for n in range(NEW):
+            p = reads_u[n * rows : (n + 1) * rows]
+            for j in range(n):
+                p = p - ps[j] * u_c[n][j] + vs[j] * u_k[n][j]
+            ps.append(p)
+            o_n = reads_q[n * rows : (n + 1) * rows]
             for j in range(n + 1):
-                o_n = o_n - ps[j] * half_sum(ct[j] * qs[n]) + vs[j] * half_sum(kt[j] * qs[n])
+                o_n = o_n - ps[j] * q_c[n][j] + vs[j] * q_k[n][j]
             mean = jnp.mean(o_n, 1, keepdims=True)
             off = o_n - mean
             var = jnp.mean(off * off, 1, keepdims=True)
-            normed = off * lax.rsqrt(var + group_epsilon) * rows_gain[b]
-            mixrel[n] = lives[n] * jax.nn.sigmoid(rel[5 * NEW + n]) * normed
+            outs.append(lives[n] * (off * lax.rsqrt(var + group_epsilon) * rows_gain[b]))
+        gates = receive(5)
+        for n in range(NEW):
+            mixrel[n] = jax.nn.sigmoid(gates[n]) * outs[n]
             for hp in range(heads // 2):
                 even = mixrel[n, pl.ds(2 * hp, seqs, stride=heads), :]
                 odd = mixrel[n, pl.ds(2 * hp + 1, seqs, stride=heads), :]
@@ -335,58 +396,96 @@
 
         wide_lane = lax.broadcasted_iota(jnp.int32, (rows, LANES), 1) < HEAD
         for i in range(NEW):
-            ship[2 * i * rows : (2 * i + 1) * rows, :] = jnp.where(wide_lane, -ps[i], 0.0).astype(
-                bf16
-            )
-            ship[(2 * i + 1) * rows : (2 * i + 2) * rows, :] = jnp.where(
+            ship[b, 2 * i * rows : (2 * i + 1) * rows, :] = jnp.where(
+                wide_lane, -ps[i], 0.0
+            ).astype(bf16)
+            ship[b, (2 * i + 1) * rows : (2 * i + 2) * rows, :] = jnp.where(
                 wide_lane, vs[i], 0.0
             ).astype(bf16)
-        step = 512
-        for j in range(flat // step):
-            spread = lax.dot_general(
-                ship[...],
-                expand[j * step : (j + 1) * step, :],
-                (((1,), (1,)), ((), ())),
-                preferred_element_type=f32,
-            )
-            for m in range(step // LANES):
-                lanes = slice(m * LANES, (m + 1) * LANES)
-                at = slice(j * step + m * LANES, j * step + (m + 1) * LANES)
-                acc = st_vm[b, :, at] * carried
-                for i in range(NEW):
-                    acc = acc + spread[2 * i * rows : (2 * i + 1) * rows, lanes] * ct[i]
-                    acc = acc + spread[(2 * i + 1) * rows : (2 * i + 2) * rows, lanes] * kt[i]
-                so_vm[b, :, at] = acc
-        pltpu.make_async_copy(so_vm.at[b], states_out.at[b], store_sem.at[b]).start()
+
+        new_state(b, 0, early[b])
 
         for copy in mix_copies:
             copy.wait_recv()
         wo_loads[b].wait()
         outp = jnp.dot(mixed[b], wo_vm[b], preferred_element_type=f32)
-        psend[b] = outp.astype(bf16).reshape(tp_n, local, feat)
-        p_copies = []
-        for o in range(1, tp_n):
-            copy = remote(
-                psend.at[b, lax.rem(t + o, tp_n)],
-                precv.at[b, o],
-                p_s.at[b, o],
-                p_r.at[b, o],
-                tp_peer(o),
-            )
-            copy.start()
-            p_copies.append(copy)
-        pending.extend(p_copies)
-        here = pl.ds(pl.multiple_of(t * local, local), local)
-        acc = psend[b, t].astype(f32)
-        for o in range(1, tp_n):
-            p_copies[o - 1].wait_recv()
-            acc = acc + precv[b, o].astype(f32)
-        fresh = (gat[b, here, :].astype(f32) + acc).astype(bf16)
+        psend[b] = outp.astype(bf16).reshape(2 * tp_n, half, feat)
         if b == 0:
-            gat[1, here, :] = fresh
-            arrivals = gather_tokens(1)
+            first = jnp.where(t >= (tp_n + 1) // 2, 1, 0)
+
+            def pass_on(way, k, last):
+                to = t + 1 - 2 * way
+                back = t - 1 + 2 * way
+                has_in = jnp.logical_and(back >= 0, back < tp_n)
+                has_out = jnp.logical_and(to >= 0, to < tp_n)
+                arrive = remote(
+                    run.at[way, k], came.at[way, k], run_s.at[way, k], run_r.at[way, k], (g, t, d)
+                )
+
+                @pl.when(has_in)
+                def _():
+                    arrive.wait_recv()
+
+                @pl.when(has_out)
+                def _():
+                    run[way, k] = (came[way, k].astype(f32) + psend[0, k].astype(f32)).astype(bf16)
+                    remote(
+                        run.at[way, k], came.at[way, k], run_s.at[way, k], run_r.at[way, k], (g, to, d)
+                    ).start()
+
+                if last:
+                    at = pl.ds(k * half, half)
+                    gat[1, at, :] = (
+                        gat[0, at, :].astype(f32)
+                        + (
+                            psend[0, k].astype(f32)
+                            + came[0, k].astype(f32)
+                            + came[1, k].astype(f32)
+                        )
+                    ).astype(bf16)
+
+            count = 2 * tp_n
+            lag = count // 2
+            for i in range(count + lag):
+                if i < count:
+                    pass_on(first, i, False)
+                if i >= lag:
+                    pass_on(1 - first, i - lag, True)
         else:
-            tokens_out[...] = fresh
+            p_copies = []
+            for o in range(1, tp_n):
+                copy = remote(
+                    psend.at[b, pl.ds(lax.rem(t + o, tp_n) * 2, 2)],
+                    precv.at[o],
+                    p_s.at[o],
+                    p_r.at[o],
+                    tp_peer(o),
+                )
+                copy.start()
+                p_copies.append(copy)
+            pending.extend(p_copies)
+            new_state(0, early[0], flat // step)
+            new_state(1, early[1], flat // step)
+            for m in range(2):
+                rows_at = pl.ds(pl.multiple_of(t * local + m * half, half), half)
+                acc = psend[b, t * 2 + m].astype(f32)
+                for o in range(1, tp_n):
+                    if m == 0:
+                        p_copies[o - 1].wait_recv()
+                    acc = acc + precv[o, m].astype(f32)
+                tokens_out[m * half : (m + 1) * half, :] = (
+                    gat[b, rows_at, :].astype(f32) + acc
+                ).astype(bf16)
+
+    for way in range(2):
+        to = t + 1 - 2 * way
+
+        @pl.when(jnp.logical_and(to >= 0, to < tp_n))
+        def _():
+            for k in range(2 * tp_n):
+                remote(
+                    run.at[way, k], came.at[way, k], run_s.at[way, k], run_r.at[way, k], (g, to, d)
+                ).wait_send()
 
     for b in range(2):
         pltpu.make_async_copy(so_vm.at[b], states_out.at[b], store_sem.at[b]).wait()
@@ -412,6 +511,8 @@
         flat = states.shape[3]
         flat_states = states.reshape(2, rows, flat)
         any_spec = pl.BlockSpec(memory_space=pl.ANY)
+        hbm_spec = pl.BlockSpec(memory_space=pltpu.HBM)
+        limit = 62500000
         vmem = pltpu.VMEM
         dma = pltpu.SemaphoreType.DMA
         tokens_out, states_out = pl.pallas_call(
@@ -420,7 +521,7 @@
                 jax.ShapeDtypeStruct((local, feat), bf16),
                 jax.ShapeDtypeStruct((2, rows, flat), f32),
             ),
-            in_specs=[any_spec, pl.BlockSpec(memory_space=pltpu.SMEM)] + [any_spec] * 11,
+            in_specs=[hbm_spec, pl.BlockSpec(memory_space=pltpu.SMEM)] + [hbm_spec] * 11,
             out_specs=(pl.BlockSpec(memory_space=pltpu.VMEM), any_spec),
             scratch_shapes=[
                 vmem((2, total, feat), bf16),
@@ -446,13 +547,18 @@
                 vmem((2, rows, LANES), f32),
                 vmem((2, rows, LANES), f32),
                 vmem((rows, LANES), f32),
-                vmem((2 * NEW * rows, flat), bf16),
+                vmem((NEW * rows, flat), bf16),
                 vmem((NEW, rows, LANES), f32),
                 vmem((heads // 2, own, LANES), f32),
                 vmem((2, total, width), bf16),
-                vmem((2, tp_n, local, feat), bf16),
-                vmem((2, tp_n, local, feat), bf16),
-                vmem((2 * NEW * rows, LANES), bf16),
+                vmem((2, 2 * tp_n, local // 2, feat), bf16),
+                vmem((tp_n, 2, local // 2, feat), bf16),
+                vmem((2, 2 * NEW * rows, LANES), bf16),
+                vmem((2, 1 + 2 * NEW, rows, LANES), f32),
+                vmem((2, 2 * tp_n, local // 2, feat), bf16),
+                vmem((2, 2 * tp_n, local // 2, feat), bf16),
+                dma((2, 2 * tp_n)),
+                dma((2, 2 * tp_n)),
                 dma((4,)),
                 dma((2, ROLES + 2)),
                 dma((2,)),
@@ -464,11 +570,11 @@
                 dma((2, ROLES + 1, chips)),
                 dma((2, dp_n)),
                 dma((2, dp_n)),
-                dma((2, tp_n)),
-                dma((2, tp_n)),
+                dma((tp_n,)),
+                dma((tp_n,)),
             ],
             compiler_params=pltpu.CompilerParams(
-                collective_id=0, has_side_effects=True, vmem_limit_bytes=60 * 1024 * 1024
+                collective_id=0, has_side_effects=True, vmem_limit_bytes=limit
             ),
         )(*args[:12], flat_states)
         return tokens_out, states_out.reshape(states.shape)

time: 72.1 us -> 81.3 us (1.13)
  Pallas kernels: 66.7 us -> 75.9 us
    pallas_call x1, Pallas kernels: 66.7 us -> 75.9 us  [per_device(): pl.pallas_call(functools.partial(kernel, tp_n, dp_n, feat * dp_n), out_sh...]
where the time goes in v1:
time: 81.3 us; the launch traced here: 81.1 us
  Pallas kernels  75.9 us (93%)
  local copies, waits for them, and re-layouts  4.58 us (6%)
    pallas_call x1, Pallas kernels, per_device(): pl.pallas_call(functools.partial(kernel, tp_n, dp_n, feat * dp_n), out_sh...  75.9 us
    unnamed x2, local copies, waits for them, and re-layouts  4.58 us

profile of v1, /device:TPU:0, one launch (start us, length us, event | category | flops | bytes accessed | tf_op | source)
XLA Modules:
  0.0 81.1 jit_solution(10354838151367772036)
XLA Ops:
  0.6 75.9 %shard_map.140 = (bf16[32,1024]{1,0:T(8,128)(2,1)}, f32[2,64,4096]{2,1,0:T(8,128)}) custom-call(bf16[32,1024]{1,0:T(8,128)(2,1)} %tokens.1, s32[8]{0:T(128)} %lengths.1, f32[2,1024]{1,0:T(2,128)} %norm_gain.1, bf16[2,1024,512]{2,1,0:T(8,128)(2,1)} %w_recept.1, bf16[2,1024,512]{2,1,0:T(8,128)(2,1)} %w_keys.1, bf16[2,1024,512]{2,1,0:T(8,128)(2,1)} %w_values.1, ...), custom_call_target="tpu_custom_call" | custom-call | tf_op jit(solution)/shard_map/pallas_call | solution.py:518
  76.5 1.5 %copy.17 = bf16[32,1024]{1,0:T(8,128)(2,1)} copy(bf16[32,1024]{1,0:T(8,128)(2,1)} %get-tuple-element.8) | data formatting | bytes 131072
  78.0 3.1 %copy.18 = f32[2,8,8,4096]{3,2,1,0:T(8,128)} copy(f32[2,8,8,4096]{3,2,1,0:T(8,128)} %bitcast.2) | data formatting | bytes 4194304

commit v2 on v1

--- a/solution.py
+++ b/solution.py
@@ -69,10 +69,6 @@
     precv,
     ship,
     factors,
-    run,
-    came,
-    run_s,
-    run_r,
     load_sem,
     w_sem,
     store_sem,
@@ -191,15 +187,7 @@
 
     half = local // 2
     step = 512
-    early = (3, 3)
-
-    @pl.when(t == 0)
-    def _():
-        came[0] = jnp.zeros(came.shape[1:], bf16)
-
-    @pl.when(t == tp_n - 1)
-    def _():
-        came[1] = jnp.zeros(came.shape[1:], bf16)
+    early = (4, 4)
 
     def half_sum(z):
         return 0.5 * jnp.sum(z, 1, keepdims=True)
@@ -224,13 +212,12 @@
                         * factors[b, 1 + NEW + i]
                     )
                 so_vm[b, :, at] = acc
-        if stop == flat // step:
+        if stop == flat // step and start < stop:
             pltpu.make_async_copy(so_vm.at[b], states_out.at[b], store_sem.at[b]).start()
 
     for b in range(2):
-        if b == 0:
-            for copy in arrivals:
-                copy.wait_recv()
+        for copy in arrivals:
+            copy.wait_recv()
         wide = gat[b].astype(f32)
         scaled[...] = (wide * gain_vm[b : b + 1, :]).astype(bf16)
         square = jnp.broadcast_to(jnp.sum(wide * wide, 1, keepdims=True), (total, LANES))
@@ -410,87 +397,70 @@
         wo_loads[b].wait()
         outp = jnp.dot(mixed[b], wo_vm[b], preferred_element_type=f32)
         psend[b] = outp.astype(bf16).reshape(2 * tp_n, half, feat)
+        p_copies = []
+        for o in range(1, tp_n):
+            copy = remote(
+                psend.at[b, pl.ds(lax.rem(t + o, tp_n) * 2, 2)],
+                precv.at[b, o],
+                p_s.at[b, o],
+                p_r.at[b, o],
+                tp_peer(o),
+            )
+            copy.start()
+            p_copies.append(copy)
+        pending.extend(p_copies)
         if b == 0:
-            first = jnp.where(t >= (tp_n + 1) // 2, 1, 0)
-
-            def pass_on(way, k, last):
-                to = t + 1 - 2 * way
-                back = t - 1 + 2 * way
-                has_in = jnp.logical_and(back >= 0, back < tp_n)
-                has_out = jnp.logical_and(to >= 0, to < tp_n)
-                arrive = remote(
-                    run.at[way, k], came.at[way, k], run_s.at[way, k], run_r.at[way, k], (g, t, d)
-                )
-
-                @pl.when(has_in)
-                def _():
-                    arrive.wait_recv()
-
-                @pl.when(has_out)
-                def _():
-                    run[way, k] = (came[way, k].astype(f32) + psend[0, k].astype(f32)).astype(bf16)
-                    remote(
-                        run.at[way, k], came.at[way, k], run_s.at[way, k], run_r.at[way, k], (g, to, d)
-                    ).start()
-
-                if last:
-                    at = pl.ds(k * half, half)
-                    gat[1, at, :] = (
-                        gat[0, at, :].astype(f32)
-                        + (
-                            psend[0, k].astype(f32)
-                            + came[0, k].astype(f32)
-                            + came[1, k].astype(f32)
-                        )
-                    ).astype(bf16)
-
-            count = 2 * tp_n
-            lag = count // 2
-            for i in range(count + lag):
-                if i < count:
-                    pass_on(first, i, False)
-                if i >= lag:
-                    pass_on(1 - first, i - lag, True)
+            new_state(0, early[0], 8)
         else:
-            p_copies = []
+            new_state(0, 8, flat // step)
+            new_state(1, early[1], flat // step)
+        for m in range(2):
+            rows_at = pl.ds(pl.multiple_of(t * local + m * half, half), half)
+            acc = psend[b, t * 2 + m].astype(f32)
             for o in range(1, tp_n):
-                copy = remote(
-                    psend.at[b, pl.ds(lax.rem(t + o, tp_n) * 2, 2)],
-                    precv.at[o],
-                    p_s.at[o],
-                    p_r.at[o],
-                    tp_peer(o),
-                )
-                copy.start()
-                p_copies.append(copy)
-            pending.extend(p_copies)
-            new_state(0, early[0], flat // step)
-            new_state(1, early[1], flat // step)
-            for m in range(2):
-                rows_at = pl.ds(pl.multiple_of(t * local + m * half, half), half)
-                acc = psend[b, t * 2 + m].astype(f32)
-                for o in range(1, tp_n):
-                    if m == 0:
-                        p_copies[o - 1].wait_recv()
-                    acc = acc + precv[o, m].astype(f32)
-                tokens_out[m * half : (m + 1) * half, :] = (
-                    gat[b, rows_at, :].astype(f32) + acc
-                ).astype(bf16)
-
-    for way in range(2):
-        to = t + 1 - 2 * way
-
-        @pl.when(jnp.logical_and(to >= 0, to < tp_n))
-        def _():
-            for k in range(2 * tp_n):
-                remote(
-                    run.at[way, k], came.at[way, k], run_s.at[way, k], run_r.at[way, k], (g, to, d)
-                ).wait_send()
+                if m == 0:
+                    p_copies[o - 1].wait_recv()
+                acc = acc + precv[b, o, m].astype(f32)
+            fresh = (gat[b, rows_at, :].astype(f32) + acc).astype(bf16)
+            if b == 0:
+                gat[1, rows_at, :] = fresh
+            else:
+                tokens_out[m * half : (m + 1) * half, :] = fresh
+        if b == 0:
+            arrivals = gather_tokens(1)
 
     for b in range(2):
         pltpu.make_async_copy(so_vm.at[b], states_out.at[b], store_sem.at[b]).wait()
     for copy in pending:
         copy.wait_send()
+
+
+def land(moved, states, moved_out, states_out, small, buf, in_sem, out_sem):
+    depth = buf.shape[1]
+    pieces = buf.shape[0] // 2
+    pairs = [
+        (
+            pltpu.make_async_copy(moved, small, in_sem.at[2 * pieces]),
+            pltpu.make_async_copy(small, moved_out, out_sem.at[2 * pieces]),
+        )
+    ]
+    for b in range(2):
+        for i in range(pieces):
+            at = pl.ds(i * depth, depth)
+            k = b * pieces + i
+            pairs.append(
+                (
+                    pltpu.make_async_copy(states.at[b, at], buf.at[k], in_sem.at[k]),
+                    pltpu.make_async_copy(buf.at[k], states_out.at[b, at], out_sem.at[k]),
+                )
+            )
+    for come, _ in pairs:
+        come.start()
+    for come, go in pairs:
+        come.wait()
+        go.start()
+    for _, go in pairs:
+        go.wait()
 
 
 def solution(mesh):
@@ -552,13 +522,9 @@
                 vmem((heads // 2, own, LANES), f32),
                 vmem((2, total, width), bf16),
                 vmem((2, 2 * tp_n, local // 2, feat), bf16),
-                vmem((tp_n, 2, local // 2, feat), bf16),
+                vmem((2, tp_n, 2, local // 2, feat), bf16),
                 vmem((2, 2 * NEW * rows, LANES), bf16),
                 vmem((2, 1 + 2 * NEW, rows, LANES), f32),
-                vmem((2, 2 * tp_n, local // 2, feat), bf16),
-                vmem((2, 2 * tp_n, local // 2, feat), bf16),
-                dma((2, 2 * tp_n)),
-                dma((2, 2 * tp_n)),
                 dma((4,)),
                 dma((2, ROLES + 2)),
                 dma((2,)),
@@ -570,13 +536,29 @@
                 dma((2, ROLES + 1, chips)),
                 dma((2, dp_n)),
                 dma((2, dp_n)),
-                dma((tp_n,)),
-                dma((tp_n,)),
+                dma((2, tp_n)),
+                dma((2, tp_n)),
             ],
             compiler_params=pltpu.CompilerParams(
                 collective_id=0, has_side_effects=True, vmem_limit_bytes=limit
             ),
         )(*args[:12], flat_states)
+        tokens_out, states_out = pl.pallas_call(
+            land,
+            out_shape=(
+                jax.ShapeDtypeStruct((local, feat), bf16),
+                jax.ShapeDtypeStruct((2, rows, flat), f32),
+            ),
+            in_specs=[any_spec] * 2,
+            out_specs=(any_spec, any_spec),
+            scratch_shapes=[
+                vmem((local, feat), bf16),
+                vmem((rows // 4, 8, flat), f32),
+                dma((rows // 4 + 1,)),
+                dma((rows // 4 + 1,)),
+            ],
+            compiler_params=pltpu.CompilerParams(vmem_limit_bytes=limit),
+        )(tokens_out, states_out)
         return tokens_out, states_out.reshape(states.shape)
 
     placed = (

time: 81.3 us -> 65.2 us (0.80)
  Pallas kernels: 75.9 us -> 64.4 us
  local copies, waits for them, and re-layouts: 4.58 us -> 0 us
    pallas_call x1, Pallas kernels: 75.9 us -> 61.8 us  [per_device(): pl.pallas_call(functools.partial(kernel, tp_n, dp_n, feat * dp_n), out_sh...]
    unnamed x2 -> x0, local copies, waits for them, and re-layouts: 4.58 us -> none
    pallas_call x0 -> x1, Pallas kernels: none -> 2.62 us  [per_device(): pl.pallas_call(land, out_shape=(jax.ShapeDtypeStruct((local, feat), bf16)...]
where the time goes in v2:
time: 65.2 us; the launch traced here: 65 us
  Pallas kernels  64.4 us (99%)
    pallas_call x1, Pallas kernels, per_device(): pl.pallas_call(functools.partial(kernel, tp_n, dp_n, feat * dp_n), out_sh...  61.8 us
    pallas_call x1, Pallas kernels, per_device(): pl.pallas_call(land, out_shape=(jax.ShapeDtypeStruct((local, feat), bf16)...  2.62 us

profile of v2, /device:TPU:0, one launch (start us, length us, event | category | flops | bytes accessed | tf_op | source)
XLA Modules:
  0.0 65.0 jit_solution(2600479502283299214)
XLA Ops:
  0.6 61.8 %shard_map.140 = (bf16[32,1024]{1,0:T(8,128)(2,1)}, f32[2,64,4096]{2,1,0:T(8,128)}) custom-call(bf16[32,1024]{1,0:T(8,128)(2,1)} %tokens.1, s32[8]{0:T(128)} %lengths.1, f32[2,1024]{1,0:T(2,128)} %norm_gain.1, bf16[2,1024,512]{2,1,0:T(8,128)(2,1)} %w_recept.1, bf16[2,1024,512]{2,1,0:T(8,128)(2,1)} %w_keys.1, bf16[2,1024,512]{2,1,0:T(8,128)(2,1)} %w_values.1, ...), custom_call_target="tpu_custom_call" | custom-call | tf_op jit(solution)/shard_map/pallas_call | solution.py:488
  62.4 2.6 %shard_map.141 = (bf16[32,1024]{1,0:T(8,128)(2,1)}, f32[2,64,4096]{2,1,0:T(8,128)}) custom-call(bf16[32,1024]{1,0:T(8,128)(2,1)} %get-tuple-element.6.moved, f32[2,64,4096]{2,1,0:T(8,128)} %get-tuple-element.7.states), custom_call_target="tpu_custom_call" | custom-call | tf_op jit(solution)/shard_map/pallas_call | solution.py:546
